TPU v7x, 32 devices: a whole 2x2x4 slice. The times are simulated.
32 devices in a mesh: sp: 16 (over z, y, x), tp: 2 (over core).
Axes of the slice: x: 2, y: 2, z: 4, core: 2. Of those that a mesh axis runs over, the one named last changes fastest.
Arguments:
- queries: bfloat16 [2048, 1024], P('sp', 'tp'), may hold values from -5 to 5
- keys: bfloat16 [2048, 1024], P('sp', 'tp'), may hold values from -5 to 5
- values: bfloat16 [2048, 1024], P('sp', 'tp'), may hold values from -5 to 5
- in_gate: float32 [8, 2048], P('tp', 'sp'), may hold values from -7 to 213
- forget_gate: float32 [8, 2048], P('tp', 'sp'), may hold values from 0 to 17
- stream: bfloat16 [2048, 2048], P('sp', 'tp'), may hold values from -24 to 24
- head_gain: float32 [1024], replicated, may hold values from 0.1 to 1.9
- out_weight: bfloat16 [1024, 2048], P(None, 'tp'), may hold values from -0.1875 to 0.1875
- norm_gain: float32 [2048], replicated, may hold values from 0.1 to 1.9
- gate_weight: bfloat16 [2048, 5632], P('sp', 'tp'), may hold values from -0.125 to 0.125
- up_weight: bfloat16 [2048, 5632], P('sp', 'tp'), may hold values from -0.125 to 0.125
- down_weight: bfloat16 [2048, 5632], P('sp', 'tp'), may hold values from -0.15625 to 0.15625
Outputs:
- layer_out: float32 [2048, 2048], P('sp', 'tp')
All inputs are finite; a program needn't handle non-finite values.
Results may differ from a plain program's by a relative error of at most 0.004.
Values may be sent and summed in bfloat16 or wider, within the bound.
A program may use at most 128 MiB of HBM per device.

v0:
```python
import jax
import jax.numpy as jnp
from jax import lax
from jax.sharding import PartitionSpec as P

D = 2048
HEAD_DIM = 128
BLOCK = 128
norm_eps = 1e-06
far_below = -1e30


def entering_state(total):
    memory, top, fall = total
    devices, here = (lax.axis_size("sp"), lax.axis_index("sp"))
    heads, rows, columns = memory.shape
    own_tops = jnp.broadcast_to(jnp.stack([top, fall])[None], (devices, 2, heads))
    tops = lax.all_to_all(own_tops, "sp", 0, 0)
    all_top, all_fall = (tops[:, 0], tops[:, 1])
    index = jnp.arange(devices)
    between = (index[None, None, :] > jnp.arange(-1, devices)[None, :, None]) & (
        index[None, None, :] < index[:, None, None]
    )
    after = jnp.sum(jnp.where(between[..., None], all_fall[None, None], 0.0), axis=2)
    reach = jnp.concatenate([jnp.zeros((1, heads), jnp.float32), all_top])[None] + after
    earlier = jnp.arange(-1, devices)[None, :, None] < index[:, None, None]
    reach = jnp.where(earlier, reach, -jnp.inf)
    top_in = jnp.max(reach, axis=1)
    share = jnp.exp(reach - top_in[:, None])[:, 1:]
    pieces = lax.all_to_all(
        jnp.transpose(memory.reshape(heads, devices, rows // devices, columns), (1, 0, 2, 3)),
        "sp",
        0,
        0,
    )
    sums = jnp.einsum("kjh,jhde->khde", share, pieces, precision=lax.Precision.HIGHEST)
    back = lax.all_to_all(sums, "sp", 0, 0)
    memory_in = jnp.transpose(back, (1, 0, 2, 3)).reshape(heads, rows, columns)
    return (memory_in, lax.dynamic_index_in_dim(top_in, here, 0, False), jnp.zeros_like(fall))


def merge_states(earlier, later):
    memory_early, top_early, fall_early = earlier
    memory_late, top_late, fall_late = later
    new_top = jnp.maximum(fall_late + top_early, top_late)
    keep_early = jnp.exp(fall_late + top_early - new_top)
    keep_late = jnp.exp(top_late - new_top)
    memory = keep_early[..., None, None] * memory_early + keep_late[..., None, None] * memory_late
    return (memory, new_top, fall_early + fall_late)


def memory_cell(queries, keys, values, in_gate, forget_gate, own_gain):
    tokens = queries.shape[0]
    local_heads = in_gate.shape[0]
    blocks = tokens // BLOCK
    key_scale = HEAD_DIM ** (-0.5)
    query_blocks = queries.reshape(blocks, BLOCK, local_heads, HEAD_DIM)
    key_blocks = keys.reshape(blocks, BLOCK, local_heads, HEAD_DIM)
    value_blocks = values.reshape(blocks, BLOCK, local_heads, HEAD_DIM)
    gate_blocks = in_gate.reshape(local_heads, blocks, BLOCK)
    cumulative = jnp.cumsum(
        jax.nn.log_sigmoid(forget_gate).reshape(local_heads, blocks, BLOCK), axis=-1
    )
    block_fall = cumulative[..., -1]
    log_weight = block_fall[..., None] - cumulative + gate_blocks
    block_top = jnp.max(log_weight, axis=-1)
    key_weight = jnp.exp(log_weight - block_top[..., None]) * key_scale
    weighted = (jnp.transpose(key_weight, (1, 2, 0))[..., None] * key_blocks).astype(jnp.bfloat16)
    block_memory = jnp.einsum(
        "nshd,nshe->nhde", weighted, value_blocks, preferred_element_type=jnp.float32
    )
    neutral = (
        jnp.zeros((local_heads, HEAD_DIM, HEAD_DIM), jnp.float32),
        jnp.full((local_heads,), far_below, jnp.float32),
        jnp.zeros((local_heads,), jnp.float32),
    )

    def advance(running, summary):
        return (merge_states(running, summary), running)

    device_total, before_block = lax.scan(
        advance, neutral, (block_memory, block_top.T, block_fall.T)
    )
    entering = entering_state(device_total)
    memory_in, top_in, fall_in = merge_states(
        jax.tree.map(lambda member: member[None], entering), before_block
    )
    causal = lax.broadcasted_iota(jnp.int32, (BLOCK, BLOCK), 0) >= lax.broadcasted_iota(
        jnp.int32, (BLOCK, BLOCK), 1
    )
    spread = cumulative[..., :, None] - cumulative[..., None, :] + gate_blocks[..., None, :]
    spread = jnp.where(causal, spread, -jnp.inf)
    carried = cumulative + top_in.T[..., None]
    row_top = jnp.maximum(carried, jnp.max(spread, axis=-1))
    decay_weight = jnp.exp(spread - row_top[..., None])
    scores = jnp.einsum(
        "nthd,nshd->hnts", query_blocks, key_blocks, preferred_element_type=jnp.float32
    )
    weights = (scores * key_scale * decay_weight).astype(jnp.bfloat16)
    inner_part = jnp.einsum(
        "hnts,nshe->nthe", weights, value_blocks, preferred_element_type=jnp.float32
    )
    outer_part = jnp.einsum(
        "nthd,nhde->nthe",
        query_blocks.astype(jnp.float32),
        memory_in,
        precision=lax.Precision.HIGHEST,
    )
    readout = (
        jnp.transpose(jnp.exp(carried - row_top), (1, 2, 0))[..., None] * outer_part + inner_part
    )
    row_scale = lax.rsqrt(jnp.mean(readout * readout, axis=-1, keepdims=True) + norm_eps)
    head_scale = own_gain.reshape(local_heads, HEAD_DIM)
    normed_heads = (readout * row_scale * head_scale).astype(jnp.bfloat16)
    return normed_heads.reshape(tokens, local_heads * HEAD_DIM)


def local(
    queries,
    keys,
    values,
    in_gate,
    forget_gate,
    stream,
    head_gain,
    out_weight,
    norm_gain,
    gate_weight,
    up_weight,
    down_weight,
):
    column_index = lax.axis_index("tp")
    local_width = queries.shape[1]
    own_gain = lax.dynamic_slice_in_dim(head_gain, column_index * local_width, local_width)
    heads_out = memory_cell(queries, keys, values, in_gate, forget_gate, own_gain)
    columns = out_weight.shape[1]
    projected = jnp.dot(
        lax.all_gather(heads_out, "tp", axis=1, tiled=True),
        out_weight,
        preferred_element_type=jnp.float32,
    )
    mixed_stream = stream.astype(jnp.float32) + projected
    squares = lax.psum(jnp.sum(mixed_stream * mixed_stream, axis=1), "tp")
    factor = lax.rsqrt(squares / D + norm_eps)
    own_norm = lax.dynamic_slice_in_dim(norm_gain, column_index * columns, columns)
    own_normed = (mixed_stream * factor[:, None] * own_norm).astype(jnp.bfloat16)
    if 2 * own_normed.size * lax.axis_size("tp") < 3 * gate_weight.size:
        channel = move_tokens(own_normed, gate_weight, up_weight, down_weight)
    else:
        channel = move_weights(own_normed, gate_weight, up_weight, down_weight)
    return mixed_stream + 0.5 * channel


def move_tokens(own_normed, gate_weight, up_weight, down_weight):
    devices = lax.axis_size("sp")
    rows, units = gate_weight.shape
    own_units = units // devices
    weights = jnp.stack([gate_weight.T, up_weight.T, down_weight.T])
    weights = weights.reshape(3, devices, own_units, rows)
    weights = lax.all_to_all(weights, "sp", 1, 2)
    weights = weights.reshape(3, own_units, devices * rows)
    half = lax.all_gather(own_normed, "sp", axis=0, tiled=True)
    normed = lax.all_gather(half, "tp", axis=1, tiled=True)
    gate_acts = jnp.einsum("td,fd->tf", normed, weights[0], preferred_element_type=jnp.float32)
    up_acts = jnp.einsum("td,fd->tf", normed, weights[1], preferred_element_type=jnp.float32)
    hidden = (jax.nn.silu(gate_acts) * up_acts).astype(jnp.bfloat16)
    terms = jnp.einsum("tf,fd->td", hidden, weights[2], preferred_element_type=jnp.float32)
    terms = lax.psum_scatter(terms.astype(jnp.bfloat16), "tp", scatter_dimension=1, tiled=True)
    return lax.psum_scatter(terms, "sp", scatter_dimension=0, tiled=True).astype(jnp.float32)


def move_weights(own_normed, gate_weight, up_weight, down_weight):
    normed = lax.all_gather(own_normed, "tp", axis=1, tiled=True)
    gate_acts = jnp.dot(
        normed,
        lax.all_gather(gate_weight, "sp", axis=0, tiled=True),
        preferred_element_type=jnp.float32,
    )
    up_acts = jnp.dot(
        normed,
        lax.all_gather(up_weight, "sp", axis=0, tiled=True),
        preferred_element_type=jnp.float32,
    )
    hidden = (jax.nn.silu(gate_acts) * up_acts).astype(jnp.bfloat16)
    channel_terms = jnp.einsum(
        "df,tf->dt",
        lax.all_gather(down_weight, "sp", axis=0, tiled=True),
        hidden,
        preferred_element_type=jnp.float32,
    )
    channel = lax.psum_scatter(
        channel_terms.astype(jnp.bfloat16), "tp", scatter_dimension=0, tiled=True
    ).astype(jnp.float32)
    return channel.T


def solution(mesh):
    return jax.shard_map(
        local,
        mesh=mesh,
        in_specs=(
            P("sp", "tp"),
            P("sp", "tp"),
            P("sp", "tp"),
            P("tp", "sp"),
            P("tp", "sp"),
            P("sp", "tp"),
            P(),
            P(None, "tp"),
            P(),
            P("sp", "tp"),
            P("sp", "tp"),
            P("sp", "tp"),
        ),
        out_specs=P("sp", "tp"),
        check_vma=False,
    )
```

profile of v0, /device:TPU:0, one launch (start us, length us, event | category | flops | bytes accessed | tf_op | source)
XLA Modules:
  0.0 339.9 jit_solution(915699007568806377)
XLA Ops:
  6.5 0.9 fusion.53
  7.4 1.2 reduce_window_sum.13
  8.7 0.1 copy.154
  8.8 0.1 copy.127
  8.9 0.9 fusion.60
  9.8 0.1 copy.128
  9.9 0.1 copy.130
  10.0 0.6 broadcast_in_dim.92
  10.7 8.3 %all-to-all-start = ((f32[16,2,4]{2,1,0:T(2,128)}), f32[16,2,4]{2,1,0:T(2,128)S(1)}, u32[]{:S(2)}, u32[]{:S(2)}) async-start(f32[16,2,4]{2,1,0:T(2,128)} %broadcast_in_dim.92), calls=%async_computation | async-start | bytes 32768 | tf_op jit(solution)/shard_map/all_to_all | solution.py:18
  19.1 0.1 broadcast_and_fusion
  19.2 0.9 select_reduce_fusion.1
  20.1 1.0 copy.155
  21.2 1.0 copy.156
  22.2 4.1 %all-to-all-done = f32[16,2,4]{2,1,0:T(2,128)S(1)} async-done(((f32[16,2,4]{2,1,0:T(2,128)}), f32[16,2,4]{2,1,0:T(2,128)S(1)}, u32[]{:S(2)}, u32[]{:S(2)}) %all-to-all-start) | async-done | bytes 544 | tf_op jit(solution)/shard_map/all_to_all | solution.py:18
  26.6 0.2 select_reduce_fusion
  26.8 0.1 fusion.61
  26.9 0.2 fusion.48
  27.1 0.8 multiply_bitcast_fusion
  27.9 0.2 convolution_bitcast_fusion.3
  28.1 0.1 fusion.20
  28.2 11.9 %all_to_all.30 = f32[16,4,8,128]{3,2,1,0:T(8,128)S(1)} all-to-all(f32[16,4,8,128]{3,2,1,0:T(8,128)S(1)} %fusion.20), channel_id=1, replica_groups=mesh['sp'=16,'tp'=2] {'sp'}, dimensions={0} | all-to-all | bytes 524288 | tf_op jit(solution)/shard_map/all_to_all | solution.py:30
  40.1 0.5 convolution_bitcast_fusion.2
  40.6 0.8 copy.138
  41.4 3.5 %all-to-all-start.2 = ((f32[16,4,8,128]{3,2,1,0:T(8,128)}), f32[16,4,8,128]{3,2,1,0:T(8,128)S(1)}, u32[]{:S(2)}, u32[]{:S(2)}) async-start(f32[16,4,8,128]{3,2,1,0:T(8,128)} %copy.138), calls=%async_computation.2 | async-start | bytes 524288 | tf_op jit(solution)/shard_map/all_to_all | solution.py:37
  45.1 0.4 convolution_bitcast_fusion.1
  45.6 8.6 %all-to-all-done.2 = f32[16,4,8,128]{3,2,1,0:T(8,128)S(1)} async-done(((f32[16,4,8,128]{3,2,1,0:T(8,128)}), f32[16,4,8,128]{3,2,1,0:T(8,128)S(1)}, u32[]{:S(2)}, u32[]{:S(2)}) %all-to-all-start.2) | async-done | bytes 262176 | tf_op jit(solution)/shard_map/all_to_all | solution.py:37
  54.2 0.5 multiply_reduce_fusion.1
  54.7 0.1 multiply_convert_fusion.1
  54.8 2.0 all_gather.9
  56.8 0.5 multiply_reduce_fusion
  57.4 2.5 psum.7
  59.9 0.8 multiply_convert_fusion
  60.7 73.6 %all-gather.3.cloned.1.call-done = bf16[2048,1024]{1,0:T(8,128)(2,1)} async-done(((bf16[128,1024]{1,0:T(8,128)(2,1)}), bf16[2048,1024]{1,0:T(8,128)(2,1)}) %all-gather.3.cloned.1.call-update) | async-done | bytes 4194320 | tf_op jit(solution)/shard_map/all_gather | solution.py:162
  134.4 1.5 copy.145
  135.9 2.3 copy.146
  138.2 2.3 copy.147
  140.4 1.8 pad_maximum_fusion
  142.2 0.1 copy.148
  142.4 54.4 %all_to_all.31 = bf16[3,16,176,1,128]{4,2,3,0,1:T(8,128)(2,1)S(1)} all-to-all(bf16[3,16,176,1,128]{4,2,3,0,1:T(8,128)(2,1)S(1)} %copy.148), channel_id=1, replica_groups=mesh['sp'=16,'tp'=2] {'sp'}, dimensions={1} | all-to-all | bytes 4325376 | tf_op jit(solution)/shard_map/all_to_all | solution.py:160
  196.7 0.1 fusion.63
  196.9 0.2 copy.150
  197.1 1.1 copy.151
  198.2 1.1 copy.149
  199.2 7.6 %fusion.11 = f32[2048,176]{0,1:T(8,128)} fusion(bf16[2048,2048]{1,0:T(8,128)(2,1)} %all-gather.5.cloned.1.call-done, bf16[22,8,16,128]{3,2,1,0:T(8,128)(2,1)} %bitcast.129), kind=kOutput, calls=%fused_computation.18 | convolution fusion | flops 1476395008 | bytes 10551296 | tf_op jit(solution)/shard_map/td,fd->tf/dot_general | solution.py:164
  206.8 12.3 %convolution_convert_fusion = bf16[2048,2048]{1,0:T(8,128)(2,1)} fusion(bf16[2048,2048]{1,0:T(8,128)(2,1)} %all-gather.5.cloned.1.call-done, f32[2048,176]{0,1:T(8,128)} %fusion.11, bf16[22,8,16,128]{3,2,1,0:T(8,128)(2,1)} %bitcast.128, bf16[22,8,16,128]{3,2,1,0:T(8,128)(2,1)S(1)} %bitcast.127), kind=kOutput, calls=%fused_computation | convolution fusion | flops 2959147008 | bytes 19660800 | tf_op jit(solution)/shard_map/tf,fd->td/dot_general | solution.py:167
  219.2 13.6 %reduce-scatter.3.cloned.1.call-done = bf16[2048,1024]{1,0:T(8,128)(2,1)} async-done(((bf16[2048,2048]{1,0:T(8,128)(2,1)}), bf16[2048,1024]{1,0:T(8,128)(2,1)}) %reduce-scatter.3.cloned.1.call-update) | async-done | bytes 4194320 | tf_op jit(solution)/shard_map/reduce_scatter | solution.py:168
  232.9 98.7 %reduce-scatter.5.cloned.1.call-done = bf16[128,1024]{1,0:T(8,128)(2,1)} async-done(((bf16[2048,1024]{1,0:T(8,128)(2,1)}), bf16[128,1024]{1,0:T(8,128)(2,1)}) %reduce-scatter.5.cloned.1.call-update) | async-done | bytes 262160 | tf_op jit(solution)/shard_map/reduce_scatter | solution.py:169
  331.6 1.8 multiply_add_fusion
  (38 shorter events, 0.9 us)
Async XLA Ops:
  6.5 50.3 %copy-start = (bf16[1024,1024]{1,0:T(8,128)(2,1)S(1)}, bf16[1024,1024]{1,0:T(8,128)(2,1)}, u32[]{:S(2)}) copy-start(bf16[1024,1024]{1,0:T(8,128)(2,1)} %param.19) | copy-start | bytes 6291460
  6.5 38.6 %copy-start.3 = (f32[4,128]{1,0:T(4,128)S(1)}, f32[4,128]{1,0:T(4,128)}, u32[]{:S(2)}) copy-start(f32[4,128]{1,0:T(4,128)} %param.15) | copy-start | bytes 6148
  6.5 38.5 %copy-start.4 = (f32[1024]{0:T(1024)S(1)}, f32[1024]{0:T(1024)}, u32[]{:S(2)}) copy-start(f32[1024]{0:T(1024)} %param.18) | copy-start | bytes 12292
  6.5 38.6 %copy-start.2 = (bf16[128,512]{1,0:T(8,128)(2,1)S(1)}, bf16[128,512]{1,0:T(8,128)(2,1)}, u32[]{:S(2)}) copy-start(bf16[128,512]{1,0:T(8,128)(2,1)} %param.12) | copy-start | bytes 393220
  10.7 15.7 %all-to-all-start = ((f32[16,2,4]{2,1,0:T(2,128)}), f32[16,2,4]{2,1,0:T(2,128)S(1)}, u32[]{:S(2)}, u32[]{:S(2)}) async-start(f32[16,2,4]{2,1,0:T(2,128)} %broadcast_in_dim.92), calls=%async_computation | async-start | bytes 32768 | tf_op jit(solution)/shard_map/all_to_all | solution.py:18
  40.1 16.7 %copy-start.1 = (bf16[128,1024]{1,0:T(8,128)(2,1)S(1)}, bf16[128,1024]{1,0:T(8,128)(2,1)}, u32[]{:S(2)}) copy-start(bf16[128,1024]{1,0:T(8,128)(2,1)} %param.17) | copy-start | bytes 786436
  41.4 12.8 %all-to-all-start.2 = ((f32[16,4,8,128]{3,2,1,0:T(8,128)}), f32[16,4,8,128]{3,2,1,0:T(8,128)S(1)}, u32[]{:S(2)}, u32[]{:S(2)}) async-start(f32[16,4,8,128]{3,2,1,0:T(8,128)} %copy.138), calls=%async_computation.2 | async-start | bytes 524288 | tf_op jit(solution)/shard_map/all_to_all | solution.py:37
  45.0 89.4 %all-gather.3.cloned.1.call-start = ((), (), s32[]{:S(2)}) async-start(), calls=%async_computation.6 | async-start | bytes 4456448 | tf_op jit(solution)/shard_map/all_gather | solution.py:162
  54.7 5.2 %dynamic-slice-start = ((f32[2048]{0:T(1024)}, s32[]{:T(128)}), f32[1024]{0:T(1024)S(1)}, s32[]{:S(2)}) async-start(f32[2048]{0:T(1024)} %param.20, s32[]{:T(128)} %select_n.44), calls=%async_computation.10 | async-start | bytes 8704 | tf_op jit(solution)/shard_map/dynamic_slice | solution.py:145
  60.7 138.5 %all-gather.5.cloned.1.call-start = ((), (), s32[]{:S(2)}) async-start(), calls=%async_computation.7 | async-start | bytes 12582912 | tf_op jit(solution)/shard_map/all_gather | solution.py:163
  134.4 98.4 %reduce-scatter.3.cloned.1.call-start = ((), (), s32[]{:S(2)}) async-start(), calls=%async_computation.8 | async-start | bytes 12582912 | tf_op jit(solution)/shard_map/reduce_scatter | solution.py:168
  219.1 112.4 %reduce-scatter.5.cloned.1.call-start = ((), (), s32[]{:S(2)}) async-start(), calls=%async_computation.9 | async-start | bytes 4456448 | tf_op jit(solution)/shard_map/reduce_scatter | solution.py:169
Sparse Core Ops, SparseCore 0:
  60.8 73.5 all-gather.2
  135.9 18.4 all-gather.4
  219.3 13.5 reduce-scatter.2
  235.0 96.5 reduce-scatter.4
where the time goes:
time: 341 us; the launch traced here: 340 us
  waiting for transfers between devices  199 us (58%)
  blocking collectives  70.7 us (21%)
  matrix products  22 us (6%)
  between operations  13.3 us (4%)
  local copies, waits for them, and re-layouts  12.9 us (4%)
  starting transfers between devices  12.1 us (4%)
  other arithmetic  10.1 us (3%)
    reduce_scatter x1, waiting for transfers between devices, move_tokens(): lax.psum_scatter(terms, 'sp', scatter_dimension=0, tiled=True)  98.7 us
    all_gather x1, waiting for transfers between devices, move_tokens(): half = lax.all_gather(own_normed, 'sp', axis=0, tiled=True)  73.6 us
    all_to_all x1, blocking collectives, move_tokens(): weights = lax.all_to_all(weights, 'sp', 1, 2)  54.4 us
    reduce_scatter x1, waiting for transfers between devices, move_tokens(): lax.psum_scatter(terms.astype(jnp.bfloat16), 'tp', scatter_dimension=1, t...  13.6 us
    dot_general x1, matrix products, move_tokens(): jnp.einsum('tf,fd->td', hidden, weights[2], preferred_element_type=jnp.fl...  12.3 us
    all_to_all x1, blocking collectives, entering_state(): lax.all_to_all(jnp.transpose(memory.reshape(heads, devices, rows // devic...  11.9 us
    all_to_all x1, waiting for transfers between devices, entering_state(): back = lax.all_to_all(sums, 'sp', 0, 0)  8.61 us
    all_to_all x1, starting transfers between devices, entering_state(): tops = lax.all_to_all(own_tops, 'sp', 0, 0)  8.34 us
  transfers between devices with their start and end apart: 6, of which 5 were waited for; matrix products, arithmetic and copies ran while one was open for 4% of the time, Pallas kernels for 0%

commit v1 on v0

--- a/solution.py
+++ b/solution.py
@@ -159,7 +159,20 @@
     weights = weights.reshape(3, devices, own_units, rows)
     weights = lax.all_to_all(weights, "sp", 1, 2)
     weights = weights.reshape(3, own_units, devices * rows)
-    half = lax.all_gather(own_normed, "sp", axis=0, tiled=True)
+    ways, here_2, step = (lax.axis_size("sp"), lax.axis_index("sp"), own_normed.shape[0])
+    lengths = [n * ways if d == 0 else n for d, n in enumerate(own_normed.shape)]
+    half = lax.dynamic_update_slice_in_dim(
+        jnp.zeros(lengths, own_normed.dtype), own_normed, here_2 * step, axis=0
+    )
+    going_up = going_down = own_normed
+    for far in range(1, ways // 2 + 1):
+        going_up = lax.ppermute(going_up, "sp", [(d, (d + 1) % ways) for d in range(ways)])
+        half = lax.dynamic_update_slice_in_dim(half, going_up, (here_2 - far) % ways * step, axis=0)
+        if 2 * far < ways:
+            going_down = lax.ppermute(going_down, "sp", [(d, (d - 1) % ways) for d in range(ways)])
+            half = lax.dynamic_update_slice_in_dim(
+                half, going_down, (here_2 + far) % ways * step, axis=0
+            )
     normed = lax.all_gather(half, "tp", axis=1, tiled=True)
     gate_acts = jnp.einsum("td,fd->tf", normed, weights[0], preferred_element_type=jnp.float32)
     up_acts = jnp.einsum("td,fd->tf", normed, weights[1], preferred_element_type=jnp.float32)

time: 341 us -> 375 us (1.100)
  starting transfers between devices: 12.1 us -> 73.2 us
  waiting for transfers between devices: 199 us -> 152 us
  local copies, waits for them, and re-layouts: 12.9 us -> 30.8 us
    all_gather x1 -> x0, waiting for transfers between devices: 73.6 us -> none  [move_tokens(): half = lax.all_gather(own_normed, 'sp', axis=0, tiled=True)]
    ppermute x0 -> x15, starting transfers between devices: none -> 61.2 us  [the longest x7 50.1 us: move_tokens(): lax.ppermute(going_down, 'sp', [(d, (d - 1) % ways) for d in range(ways)])]
    ppermute x0 -> x15, waiting for transfers between devices: none -> 28.6 us  [the longest x8 20 us: move_tokens(): lax.ppermute(going_up, 'sp', [(d, (d + 1) % ways) for d in range(ways)])]
    dynamic_update_slice x0 -> x15, local copies, waits for them, and re-layouts: none -> 14.6 us  [the longest x8 7.66 us: move_tokens(): lax.dynamic_update_slice_in_dim(half, going_up, (here_2 - far) % ways * s...]
  transfers between devices with their start and end apart: 6 -> 20, of which waited for: 5 -> 13; matrix products, arithmetic and copies ran while one was open for 4% -> 8% of each run, Pallas kernels for 0% -> 0%
where the time goes in v1:
time: 375 us; the launch traced here: 374 us
  waiting for transfers between devices  152 us (41%)
  starting transfers between devices  73.2 us (20%)
  blocking collectives  69.4 us (19%)
  local copies, waits for them, and re-layouts  30.8 us (8%)
  matrix products  23.6 us (6%)
  between operations  13.3 us (4%)
  other arithmetic  11.3 us (3%)
    reduce_scatter x1, waiting for transfers between devices, move_tokens(): lax.psum_scatter(terms, 'sp', scatter_dimension=0, tiled=True)  98.9 us
    all_to_all x1, blocking collectives, move_tokens(): weights = lax.all_to_all(weights, 'sp', 1, 2)  53.1 us
    ppermute x7, starting transfers between devices, move_tokens(): lax.ppermute(going_down, 'sp', [(d, (d - 1) % ways) for d in range(ways)])  50.1 us
    ppermute x8, waiting for transfers between devices, move_tokens(): lax.ppermute(going_up, 'sp', [(d, (d + 1) % ways) for d in range(ways)])  20 us
    reduce_scatter x1, waiting for transfers between devices, move_tokens(): lax.psum_scatter(terms.astype(jnp.bfloat16), 'tp', scatter_dimension=1, t...  13.7 us
    dot_general x1, matrix products, move_tokens(): jnp.einsum('tf,fd->td', hidden, weights[2], preferred_element_type=jnp.fl...  12.4 us
    all_to_all x1, blocking collectives, entering_state(): lax.all_to_all(jnp.transpose(memory.reshape(heads, devices, rows // devic...  11.9 us
    ppermute x8, starting transfers between devices, move_tokens(): lax.ppermute(going_up, 'sp', [(d, (d + 1) % ways) for d in range(ways)])  11.1 us
  transfers between devices with their start and end apart: 20, of which 13 were waited for; matrix products, arithmetic and copies ran while one was open for 8% of the time, Pallas kernels for 0%

profile of v1, /device:TPU:0, one launch (start us, length us, event | category | flops | bytes accessed | tf_op | source)
XLA Modules:
  0.0 374.1 jit_solution(8075566663603124749)
XLA Ops:
  7.4 1.2 reduce_window_sum.13
  10.6 8.3 %all-to-all-start = ((f32[16,2,4]{2,1,0:T(2,128)}), f32[16,2,4]{2,1,0:T(2,128)S(1)}, u32[]{:S(2)}, u32[]{:S(2)}) async-start(f32[16,2,4]{2,1,0:T(2,128)} %broadcast_in_dim.95), calls=%async_computation | async-start | bytes 32768 | tf_op jit(solution)/shard_map/all_to_all | solution.py:18
  21.2 1.0 copy.156
  22.2 4.1 %all-to-all-done = f32[16,2,4]{2,1,0:T(2,128)S(1)} async-done(((f32[16,2,4]{2,1,0:T(2,128)}), f32[16,2,4]{2,1,0:T(2,128)S(1)}, u32[]{:S(2)}, u32[]{:S(2)}) %all-to-all-start) | async-done | bytes 544 | tf_op jit(solution)/shard_map/all_to_all | solution.py:18
  27.7 1.3 multiply_bitcast_fusion
  29.3 11.9 %all_to_all.30 = f32[16,4,8,128]{3,2,1,0:T(8,128)S(1)} all-to-all(f32[16,4,8,128]{3,2,1,0:T(8,128)S(1)} %fusion.23), channel_id=1, replica_groups=mesh['sp'=16,'tp'=2] {'sp'}, dimensions={0} | all-to-all | bytes 524288 | tf_op jit(solution)/shard_map/all_to_all | solution.py:30
  42.5 3.5 all-to-all-start.2
  46.9 1.3 convolution_bitcast_fusion.1
  48.3 7.0 %all-to-all-done.2 = f32[16,4,8,128]{3,2,1,0:T(8,128)S(1)} async-done(((f32[16,4,8,128]{3,2,1,0:T(8,128)}), f32[16,4,8,128]{3,2,1,0:T(8,128)S(1)}, u32[]{:S(2)}, u32[]{:S(2)}) %all-to-all-start.2) | async-done | bytes 262176 | tf_op jit(solution)/shard_map/all_to_all | solution.py:37
  55.3 1.1 multiply_reduce_fusion.1
  56.6 2.0 all_gather.6
  59.2 2.5 psum.7
  61.6 2.5 broadcast_in_dim.107
  65.7 4.9 %collective-permute-start.1 = (bf16[128,1024]{1,0:T(8,128)(2,1)S(1)}, bf16[128,1024]{1,0:T(8,128)(2,1)S(1)}, u32[]{:S(2)}, u32[]{:S(2)}) collective-permute-start(bf16[128,1024]{1,0:T(8,128)(2,1)S(1)} %get-tuple-element.27), channel_id=1, source_target_pairs={{0,30},{2,0},{4,2},{6,4},{8,6},{10,8},{12,10},{14,12},{16,14},{18,... | collective-permute-start | bytes 786440 | tf_op jit(solution)/shard_map/ppermute | solution.py:172
  70.6 6.6 %collective-permute-done = bf16[128,1024]{1,0:T(8,128)(2,1)S(1)} collective-permute-done((bf16[128,1024]{1,0:T(8,128)(2,1)S(1)}, bf16[128,1024]{1,0:T(8,128)(2,1)S(1)}, u32[]{:S(2)}, u32[]{:S(2)}) %collective-permute-start) | collective-permute-done | bytes 262176 | tf_op jit(solution)/shard_map/ppermute | solution.py:169
  77.3 2.5 collective-permute-start.2
  79.7 7.4 %collective-permute-start.3 = (bf16[128,1024]{1,0:T(8,128)(2,1)S(1)}, bf16[128,1024]{1,0:T(8,128)(2,1)}, u32[]{:S(2)}, u32[]{:S(2)}) collective-permute-start(bf16[128,1024]{1,0:T(8,128)(2,1)S(1)} %collective-permute-done.1), channel_id=1, source_target_pairs={{0,30},{2,0},{4,2},{6,4},{8,6},{10,8},{12,10},{14,12},{16,14},{18,... | collective-permute-start | bytes 786440 | tf_op jit(solution)/shard_map/ppermute | solution.py:172
  87.2 3.2 collective-permute-done.2
  90.4 2.5 collective-permute-start.4
  92.9 6.8 %collective-permute-start.5 = (bf16[128,1024]{1,0:T(8,128)(2,1)}, bf16[128,1024]{1,0:T(8,128)(2,1)S(1)}, u32[]{:S(2)}, u32[]{:S(2)}) collective-permute-start(bf16[128,1024]{1,0:T(8,128)(2,1)} %collective-permute-done.3), channel_id=1, source_target_pairs={{0,30},{2,0},{4,2},{6,4},{8,6},{10,8},{12,10},{14,12},{16,14},{18,... | collective-permute-start | bytes 786440 | tf_op jit(solution)/shard_map/ppermute | solution.py:172
  99.7 3.2 collective-permute-done.4
  103.0 2.6 collective-permute-start.6
  105.6 1.7 constant_dynamic-update-slice_fusion.14
  107.2 5.8 %collective-permute-start.7 = (bf16[128,1024]{1,0:T(8,128)(2,1)S(1)}, bf16[128,1024]{1,0:T(8,128)(2,1)S(1)}, u32[]{:S(2)}, u32[]{:S(2)}) collective-permute-start(bf16[128,1024]{1,0:T(8,128)(2,1)S(1)} %collective-permute-done.5), channel_id=1, source_target_pairs={{0,30},{2,0},{4,2},{6,4},{8,6},{10,8},{12,10},{14,12},{16,14},{18,... | collective-permute-start | bytes 786440 | tf_op jit(solution)/shard_map/ppermute | solution.py:172
  113.0 1.7 constant_dynamic-update-slice_fusion.13
  114.7 1.1 collective-permute-done.6
  115.8 2.4 collective-permute-start.8
  118.9 1.7 constant_dynamic-update-slice_fusion.11
  120.6 7.5 %collective-permute-start.9 = (bf16[128,1024]{1,0:T(8,128)(2,1)S(1)}, bf16[128,1024]{1,0:T(8,128)(2,1)S(1)}, u32[]{:S(2)}, u32[]{:S(2)}) collective-permute-start(bf16[128,1024]{1,0:T(8,128)(2,1)S(1)} %collective-permute-done.7), channel_id=1, source_target_pairs={{0,30},{2,0},{4,2},{6,4},{8,6},{10,8},{12,10},{14,12},{16,14},{18,... | collective-permute-start | bytes 786440 | tf_op jit(solution)/shard_map/ppermute | solution.py:172
  128.1 1.7 constant_dynamic-update-slice_fusion.10
  131.6 2.2 collective-permute-done.9
  133.8 9.6 %collective-permute-start.11 = (bf16[128,1024]{1,0:T(8,128)(2,1)S(1)}, bf16[128,1024]{1,0:T(8,128)(2,1)S(1)}, u32[]{:S(2)}, u32[]{:S(2)}) collective-permute-start(bf16[128,1024]{1,0:T(8,128)(2,1)S(1)} %collective-permute-done.9), channel_id=1, source_target_pairs={{0,30},{2,0},{4,2},{6,4},{8,6},{10,8},{12,10},{14,12},{16,14},{18,... | collective-permute-start | bytes 786440 | tf_op jit(solution)/shard_map/ppermute | solution.py:172
  145.6 3.6 collective-permute-done.11
  149.2 8.1 %collective-permute-start.13 = (bf16[128,1024]{1,0:T(8,128)(2,1)S(1)}, bf16[128,1024]{1,0:T(8,128)(2,1)S(1)}, u32[]{:S(2)}, u32[]{:S(2)}) collective-permute-start(bf16[128,1024]{1,0:T(8,128)(2,1)S(1)} %collective-permute-done.11), channel_id=1, source_target_pairs={{0,30},{2,0},{4,2},{6,4},{8,6},{10,8},{12,10},{14,12},{16,14},{18,... | collective-permute-start | bytes 786440 | tf_op jit(solution)/shard_map/ppermute | solution.py:172
  159.5 2.7 collective-permute-done.13
  162.9 5.8 %collective-permute-done.14 = bf16[128,1024]{1,0:T(8,128)(2,1)S(1)} collective-permute-done((bf16[128,1024]{1,0:T(8,128)(2,1)S(1)}, bf16[128,1024]{1,0:T(8,128)(2,1)S(1)}, u32[]{:S(2)}, u32[]{:S(2)}) %collective-permute-start.14) | collective-permute-done | bytes 262176 | tf_op jit(solution)/shard_map/ppermute | solution.py:169
  169.5 1.5 copy.145
  171.0 2.2 copy.146
  173.2 2.4 copy.147
  175.6 1.8 pad_maximum_fusion
  177.6 53.1 %all_to_all.31 = bf16[3,16,176,1,128]{4,2,3,0,1:T(8,128)(2,1)S(1)} all-to-all(bf16[3,16,176,1,128]{4,2,3,0,1:T(8,128)(2,1)S(1)} %copy.148), channel_id=1, replica_groups=mesh['sp'=16,'tp'=2] {'sp'}, dimensions={1} | all-to-all | bytes 4325376 | tf_op jit(solution)/shard_map/all_to_all | solution.py:160
  231.0 1.1 copy.151
  232.1 1.1 copy.149
  233.2 7.6 %fusion.14 = f32[2048,176]{0,1:T(8,128)} fusion(bf16[2048,2048]{1,0:T(8,128)(2,1)} %all-gather.2.cloned.1.call-done, bf16[22,8,16,128]{3,2,1,0:T(8,128)(2,1)} %bitcast.132), kind=kOutput, calls=%fused_computation.18 | convolution fusion | flops 1476395008 | bytes 10551296 | tf_op jit(solution)/shard_map/td,fd->tf/dot_general | solution.py:177
  240.7 12.4 %convolution_convert_fusion = bf16[2048,2048]{1,0:T(8,128)(2,1)} fusion(f32[2048,176]{0,1:T(8,128)} %fusion.14, bf16[22,8,16,128]{3,2,1,0:T(8,128)(2,1)} %bitcast.131, bf16[2048,2048]{1,0:T(8,128)(2,1)} %all-gather.2.cloned.1.call-done, bf16[22,8,16,128]{3,2,1,0:T(8,128)(2,1)S(1)} %bitcast.130), kind=kOutput, calls=%fused_computation | convolution fusion | flops 2959147008 | bytes 19660800 | tf_op jit(solution)/shard_map/tf,fd->td/dot_general | solution.py:180
  253.2 13.7 %reduce-scatter.3.cloned.1.call-done = bf16[2048,1024]{1,0:T(8,128)(2,1)} async-done(((bf16[2048,2048]{1,0:T(8,128)(2,1)}), bf16[2048,1024]{1,0:T(8,128)(2,1)}) %reduce-scatter.3.cloned.1.call-update) | async-done | bytes 4194320 | tf_op jit(solution)/shard_map/reduce_scatter | solution.py:181
  266.9 98.9 %reduce-scatter.5.cloned.1.call-done = bf16[128,1024]{1,0:T(8,128)(2,1)} async-done(((bf16[2048,1024]{1,0:T(8,128)(2,1)}), bf16[128,1024]{1,0:T(8,128)(2,1)}) %reduce-scatter.5.cloned.1.call-update) | async-done | bytes 262160 | tf_op jit(solution)/shard_map/reduce_scatter | solution.py:182
  365.8 1.8 multiply_add_fusion
  (83 shorter events, 20.1 us)
Async XLA Ops:
  6.5 52.1 %copy-start = (bf16[1024,1024]{1,0:T(8,128)(2,1)S(1)}, bf16[1024,1024]{1,0:T(8,128)(2,1)}, u32[]{:S(2)}) copy-start(bf16[1024,1024]{1,0:T(8,128)(2,1)} %param.19) | copy-start | bytes 6291460
  6.5 48.8 %copy-start.4 = (bf16[128,512]{1,0:T(8,128)(2,1)S(1)}, bf16[128,512]{1,0:T(8,128)(2,1)}, u32[]{:S(2)}) copy-start(bf16[128,512]{1,0:T(8,128)(2,1)} %param.12) | copy-start | bytes 393220
  6.5 52.1 %copy-start.3 = (bf16[128,1024]{1,0:T(8,128)(2,1)S(1)}, bf16[128,1024]{1,0:T(8,128)(2,1)}, u32[]{:S(2)}) copy-start(bf16[128,1024]{1,0:T(8,128)(2,1)} %param.17) | copy-start | bytes 786436
  10.6 15.7 %all-to-all-start = ((f32[16,2,4]{2,1,0:T(2,128)}), f32[16,2,4]{2,1,0:T(2,128)S(1)}, u32[]{:S(2)}, u32[]{:S(2)}) async-start(f32[16,2,4]{2,1,0:T(2,128)} %broadcast_in_dim.95), calls=%async_computation | async-start | bytes 32768 | tf_op jit(solution)/shard_map/all_to_all | solution.py:18
  19.1 7.5 %copy-start.5 = (pred[128,128]{1,0:T(8,128)(4,1)}, pred[128,128]{1,0:T(8,128)(4,1)S(1)}, u32[]{:S(2)}) copy-start(pred[128,128]{1,0:T(8,128)(4,1)S(1)} %iota_compare_fusion) | copy-start | bytes 49156
  42.5 12.8 %all-to-all-start.2 = ((f32[16,4,8,128]{3,2,1,0:T(8,128)}), f32[16,4,8,128]{3,2,1,0:T(8,128)S(1)}, u32[]{:S(2)}, u32[]{:S(2)}) async-start(f32[16,4,8,128]{3,2,1,0:T(8,128)} %copy.138), calls=%async_computation.2 | async-start | bytes 524288 | tf_op jit(solution)/shard_map/all_to_all | solution.py:37
  46.1 187.1 %all-gather.2.cloned.1.call-start = ((), (), s32[]{:S(2)}) async-start(), calls=%async_computation.6 | async-start | bytes 12582912 | tf_op jit(solution)/shard_map/all_gather | solution.py:176
  56.4 7.7 %dynamic-slice-start = ((f32[2048]{0:T(1024)}, s32[]{:T(128)}), f32[1024]{0:T(1024)S(1)}, s32[]{:S(2)}) async-start(f32[2048]{0:T(1024)} %param.20, s32[]{:T(128)} %select_n.155), calls=%async_computation.9 | async-start | bytes 8704 | tf_op jit(solution)/shard_map/dynamic_slice | solution.py:145
  65.0 12.3 %collective-permute-start = (bf16[128,1024]{1,0:T(8,128)(2,1)S(1)}, bf16[128,1024]{1,0:T(8,128)(2,1)S(1)}, u32[]{:S(2)}, u32[]{:S(2)}) collective-permute-start(bf16[128,1024]{1,0:T(8,128)(2,1)S(1)} %get-tuple-element.27), channel_id=1, source_target_pairs={{0,2},{2,4},{4,6},{6,8},{8,10},{10,12},{12,14},{14,16},{16,18},{18... | collective-permute-start | bytes 786440 | tf_op jit(solution)/shard_map/ppermute | solution.py:169
  65.7 14.0 %collective-permute-start.1 = (bf16[128,1024]{1,0:T(8,128)(2,1)S(1)}, bf16[128,1024]{1,0:T(8,128)(2,1)S(1)}, u32[]{:S(2)}, u32[]{:S(2)}) collective-permute-start(bf16[128,1024]{1,0:T(8,128)(2,1)S(1)} %get-tuple-element.27), channel_id=1, source_target_pairs={{0,30},{2,0},{4,2},{6,4},{8,6},{10,8},{12,10},{14,12},{16,14},{18,... | collective-permute-start | bytes 786440 | tf_op jit(solution)/shard_map/ppermute | solution.py:172
  77.3 25.7 %copy-start.2 = (bf16[128,1024]{1,0:T(8,128)(2,1)}, bf16[128,1024]{1,0:T(8,128)(2,1)S(1)}, u32[]{:S(2)}) copy-start(bf16[128,1024]{1,0:T(8,128)(2,1)S(1)} %collective-permute-done) | copy-start | bytes 786436
  77.3 13.1 %collective-permute-start.2 = (bf16[128,1024]{1,0:T(8,128)(2,1)S(1)}, bf16[128,1024]{1,0:T(8,128)(2,1)S(1)}, u32[]{:S(2)}, u32[]{:S(2)}) collective-permute-start(bf16[128,1024]{1,0:T(8,128)(2,1)S(1)} %collective-permute-done), channel_id=1, source_target_pairs={{0,2},{2,4},{4,6},{6,8},{8,10},{10,12},{12,14},{14,16},{16,18},{18... | collective-permute-start | bytes 786440 | tf_op jit(solution)/shard_map/ppermute | solution.py:169
  79.7 23.2 %copy-start.1 = (bf16[128,1024]{1,0:T(8,128)(2,1)}, bf16[128,1024]{1,0:T(8,128)(2,1)S(1)}, u32[]{:S(2)}) copy-start(bf16[128,1024]{1,0:T(8,128)(2,1)S(1)} %collective-permute-done.1) | copy-start | bytes 786436
  79.7 13.2 %collective-permute-start.3 = (bf16[128,1024]{1,0:T(8,128)(2,1)S(1)}, bf16[128,1024]{1,0:T(8,128)(2,1)}, u32[]{:S(2)}, u32[]{:S(2)}) collective-permute-start(bf16[128,1024]{1,0:T(8,128)(2,1)S(1)} %collective-permute-done.1), channel_id=1, source_target_pairs={{0,30},{2,0},{4,2},{6,4},{8,6},{10,8},{12,10},{14,12},{16,14},{18,... | collective-permute-start | bytes 786440 | tf_op jit(solution)/shard_map/ppermute | solution.py:172
  90.4 12.6 %collective-permute-start.4 = (bf16[128,1024]{1,0:T(8,128)(2,1)S(1)}, bf16[128,1024]{1,0:T(8,128)(2,1)}, u32[]{:S(2)}, u32[]{:S(2)}) collective-permute-start(bf16[128,1024]{1,0:T(8,128)(2,1)S(1)} %collective-permute-done.2), channel_id=1, source_target_pairs={{0,2},{2,4},{4,6},{6,8},{8,10},{10,12},{12,14},{14,16},{16,18},{18... | collective-permute-start | bytes 786440 | tf_op jit(solution)/shard_map/ppermute | solution.py:169
  92.9 14.3 %collective-permute-start.5 = (bf16[128,1024]{1,0:T(8,128)(2,1)}, bf16[128,1024]{1,0:T(8,128)(2,1)S(1)}, u32[]{:S(2)}, u32[]{:S(2)}) collective-permute-start(bf16[128,1024]{1,0:T(8,128)(2,1)} %collective-permute-done.3), channel_id=1, source_target_pairs={{0,30},{2,0},{4,2},{6,4},{8,6},{10,8},{12,10},{14,12},{16,14},{18,... | collective-permute-start | bytes 786440 | tf_op jit(solution)/shard_map/ppermute | solution.py:172
  103.0 12.8 %collective-permute-start.6 = (bf16[128,1024]{1,0:T(8,128)(2,1)}, bf16[128,1024]{1,0:T(8,128)(2,1)S(1)}, u32[]{:S(2)}, u32[]{:S(2)}) collective-permute-start(bf16[128,1024]{1,0:T(8,128)(2,1)} %collective-permute-done.4), channel_id=1, source_target_pairs={{0,2},{2,4},{4,6},{6,8},{8,10},{10,12},{12,14},{14,16},{16,18},{18... | collective-permute-start | bytes 786440 | tf_op jit(solution)/shard_map/ppermute | solution.py:169
  107.2 13.3 %collective-permute-start.7 = (bf16[128,1024]{1,0:T(8,128)(2,1)S(1)}, bf16[128,1024]{1,0:T(8,128)(2,1)S(1)}, u32[]{:S(2)}, u32[]{:S(2)}) collective-permute-start(bf16[128,1024]{1,0:T(8,128)(2,1)S(1)} %collective-permute-done.5), channel_id=1, source_target_pairs={{0,30},{2,0},{4,2},{6,4},{8,6},{10,8},{12,10},{14,12},{16,14},{18,... | collective-permute-start | bytes 786440 | tf_op jit(solution)/shard_map/ppermute | solution.py:172
  115.8 14.0 %collective-permute-start.8 = (bf16[128,1024]{1,0:T(8,128)(2,1)S(1)}, bf16[128,1024]{1,0:T(8,128)(2,1)S(1)}, u32[]{:S(2)}, u32[]{:S(2)}) collective-permute-start(bf16[128,1024]{1,0:T(8,128)(2,1)S(1)} %collective-permute-done.6), channel_id=1, source_target_pairs={{0,2},{2,4},{4,6},{6,8},{8,10},{10,12},{12,14},{14,16},{16,18},{18... | collective-permute-start | bytes 786440 | tf_op jit(solution)/shard_map/ppermute | solution.py:169
  120.6 13.3 %collective-permute-start.9 = (bf16[128,1024]{1,0:T(8,128)(2,1)S(1)}, bf16[128,1024]{1,0:T(8,128)(2,1)S(1)}, u32[]{:S(2)}, u32[]{:S(2)}) collective-permute-start(bf16[128,1024]{1,0:T(8,128)(2,1)S(1)} %collective-permute-done.7), channel_id=1, source_target_pairs={{0,30},{2,0},{4,2},{6,4},{8,6},{10,8},{12,10},{14,12},{16,14},{18,... | collective-permute-start | bytes 786440 | tf_op jit(solution)/shard_map/ppermute | solution.py:172
  129.8 14.4 %collective-permute-start.10 = (bf16[128,1024]{1,0:T(8,128)(2,1)S(1)}, bf16[128,1024]{1,0:T(8,128)(2,1)S(1)}, u32[]{:S(2)}, u32[]{:S(2)}) collective-permute-start(bf16[128,1024]{1,0:T(8,128)(2,1)S(1)} %collective-permute-done.8), channel_id=1, source_target_pairs={{0,2},{2,4},{4,6},{6,8},{8,10},{10,12},{12,14},{14,16},{16,18},{18... | collective-permute-start | bytes 786440 | tf_op jit(solution)/shard_map/ppermute | solution.py:169
  133.8 15.4 %collective-permute-start.11 = (bf16[128,1024]{1,0:T(8,128)(2,1)S(1)}, bf16[128,1024]{1,0:T(8,128)(2,1)S(1)}, u32[]{:S(2)}, u32[]{:S(2)}) collective-permute-start(bf16[128,1024]{1,0:T(8,128)(2,1)S(1)} %collective-permute-done.9), channel_id=1, source_target_pairs={{0,30},{2,0},{4,2},{6,4},{8,6},{10,8},{12,10},{14,12},{16,14},{18,... | collective-permute-start | bytes 786440 | tf_op jit(solution)/shard_map/ppermute | solution.py:172
  144.2 13.9 %collective-permute-start.12 = (bf16[128,1024]{1,0:T(8,128)(2,1)S(1)}, bf16[128,1024]{1,0:T(8,128)(2,1)S(1)}, u32[]{:S(2)}, u32[]{:S(2)}) collective-permute-start(bf16[128,1024]{1,0:T(8,128)(2,1)S(1)} %collective-permute-done.10), channel_id=1, source_target_pairs={{0,2},{2,4},{4,6},{6,8},{8,10},{10,12},{12,14},{14,16},{16,18},{18... | collective-permute-start | bytes 786440 | tf_op jit(solution)/shard_map/ppermute | solution.py:169
  149.2 13.0 %collective-permute-start.13 = (bf16[128,1024]{1,0:T(8,128)(2,1)S(1)}, bf16[128,1024]{1,0:T(8,128)(2,1)S(1)}, u32[]{:S(2)}, u32[]{:S(2)}) collective-permute-start(bf16[128,1024]{1,0:T(8,128)(2,1)S(1)} %collective-permute-done.11), channel_id=1, source_target_pairs={{0,30},{2,0},{4,2},{6,4},{8,6},{10,8},{12,10},{14,12},{16,14},{18,... | collective-permute-start | bytes 786440 | tf_op jit(solution)/shard_map/ppermute | solution.py:172
  158.0 10.7 %collective-permute-start.14 = (bf16[128,1024]{1,0:T(8,128)(2,1)S(1)}, bf16[128,1024]{1,0:T(8,128)(2,1)S(1)}, u32[]{:S(2)}, u32[]{:S(2)}) collective-permute-start(bf16[128,1024]{1,0:T(8,128)(2,1)S(1)} %collective-permute-done.12), channel_id=1, source_target_pairs={{0,2},{2,4},{4,6},{6,8},{8,10},{10,12},{12,14},{14,16},{16,18},{18... | collective-permute-start | bytes 786440 | tf_op jit(solution)/shard_map/ppermute | solution.py:169
  169.5 97.4 %reduce-scatter.3.cloned.1.call-start = ((), (), s32[]{:S(2)}) async-start(), calls=%async_computation.7 | async-start | bytes 12582912 | tf_op jit(solution)/shard_map/reduce_scatter | solution.py:181
  253.1 112.7 %reduce-scatter.5.cloned.1.call-start = ((), (), s32[]{:S(2)}) async-start(), calls=%async_computation.8 | async-start | bytes 4456448 | tf_op jit(solution)/shard_map/reduce_scatter | solution.py:182
Sparse Core Ops, SparseCore 0:
  169.6 17.9 all-gather.1
  253.2 13.6 reduce-scatter.2
  269.2 96.5 reduce-scatter.4
